TPU v7x, 32 devices: a whole 2x2x4 slice. The times are simulated.
32 devices in a mesh: sp: 8 (over z, y), tp: 4 (over x, core).
Axes of the slice: x: 2, y: 2, z: 4, core: 2. Of those that a mesh axis runs over, the one named last changes fastest.
Arguments:
- query: bfloat16 [4096, 1024], P('sp', 'tp'), may hold values from -6 to 6
- key: bfloat16 [4096, 1024], P('sp', 'tp'), may hold values from -6 to 6
- value: bfloat16 [4096, 1024], P('sp', 'tp'), may hold values from -6 to 6
- out_grad: bfloat16 [4096, 1024], P('sp', 'tp'), may hold values from -6 to 6
- query_gain: float32 [64], replicated, may hold values from 0.1 to 1.9
- key_gain: float32 [64], replicated, may hold values from 0.1 to 1.9
- rel_bias: float32 [16, 129], P('tp'), may hold values from -3 to 3
Outputs:
- query_grad: bfloat16 [4096, 1024], P('sp', 'tp')
- key_grad: bfloat16 [4096, 1024], P('sp', 'tp')
- value_grad: bfloat16 [4096, 1024], P('sp', 'tp')
- query_gain_grad: float32 [64], replicated
- key_gain_grad: float32 [64], replicated
- bias_grad: float32 [16, 129], P('tp')
All inputs are finite; a program needn't handle non-finite values.
Results may differ from a plain program's by a relative error of at most 0.0095.
Values may be sent and summed in bfloat16 or wider, within the bound.
A program may use at most 64 MiB of HBM per device.

v0:
```python
import functools

import jax
import jax.numpy as jnp
from jax import lax
from jax.experimental import pallas as pl
from jax.experimental.pallas import tpu as pltpu
from jax.sharding import PartitionSpec as P

CLIP = 128
TILE = 128
LANES = 128
WIDE = 2 * TILE
EPSILON = 1e-06
LOG2E = 1.4426950408889634
MASKED = -1e30
MESH = pl.DeviceIdType.MESH
NT = (((1,), (1,)), ((), ()))
NN = (((1,), (0,)), ((), ()))


def dot(a, b, dims=NN):
    return lax.dot_general(a, b, dims, preferred_element_type=jnp.float32)


def iota(shape, axis):
    return lax.broadcasted_iota(jnp.int32, shape, axis)


def half_mean(x):
    low = iota(x.shape, 1) < LANES // 2
    first = jnp.sum(jnp.where(low, x, 0.0), axis=1, keepdims=True)
    second = jnp.sum(jnp.where(low, 0.0, x), axis=1, keepdims=True)
    return jnp.where(low, first, second) * (2.0 / LANES)


def unit_of(x):
    scale = lax.rsqrt(half_mean(x * x) + EPSILON)
    return x * scale, scale


def skew(x, left):
    row = iota(x.shape, 0)
    for bit in range(7):
        step = 1 << bit
        moved = pltpu.roll(x, LANES - step if left else step, 1)
        x = jnp.where((row & step) != 0, moved, x)
    return x


def kernel(
    axis_sizes,
    head_width,
    q_hbm,
    k_hbm,
    v_hbm,
    g_hbm,
    q_gain_ref,
    k_gain_ref,
    bias_ref,
    q_out_hbm,
    k_out_hbm,
    v_out_hbm,
    q_gain_out,
    k_gain_out,
    bias_out,
    q_ref,
    k_ref,
    v_ref,
    g_ref,
    q_out,
    k_out,
    v_out,
    next_q,
    next_g,
    stat_send,
    stat_recv,
    norm_send,
    norm_recv,
    dq_send,
    dq_recv,
    k_hat,
    k_turned,
    own_q,
    own_g,
    far_q,
    far_g,
    own_e,
    own_p,
    far_e,
    far_p,
    dk,
    dv,
    dq_own,
    near_bias,
    taps,
    totals,
    own_stat,
    q_unit,
    q_scale,
    next_unit,
    k_unit,
    k_scale,
    gain_part,
    message,
    gathered,
    gain_message,
    gain_gathered,
    in_send_sem,
    in_recv_sem,
    stat_send_sem,
    stat_recv_sem,
    norm_send_sem,
    norm_recv_sem,
    dq_send_sem,
    dq_recv_sem,
    sum_send_sem,
    sum_recv_sem,
    gain_send_sem,
    gain_recv_sem,
    load_sem,
    store_sem,
):
    n_sp, n_tp = axis_sizes
    rows, width = q_hbm.shape
    tiles = rows // TILE
    pairs = width // LANES
    heads = 2 * pairs
    score_scale = head_width ** (-0.5)
    me = lax.axis_index("sp")
    me_tp = lax.axis_index("tp")
    has_prev = me > 0
    has_next = me < n_sp - 1
    before = jnp.maximum(me - 1, 0)
    after = jnp.minimum(me + 1, n_sp - 1)

    def span(t):
        return slice(t * TILE, (t + 1) * TILE)

    def pair_lanes(p):
        return slice(p * LANES, (p + 1) * LANES)

    def copy(src, dst, send, recv, target):
        return pltpu.make_async_remote_copy(
            src_ref=src,
            dst_ref=dst,
            send_sem=send,
            recv_sem=recv,
            device_id={"sp": target},
            device_id_type=MESH,
        )

    def in_copies(t):
        return (
            copy(q_ref.at[span(t)], next_q.at[span(t)], in_send_sem.at[2 * t], in_recv_sem.at[2 * t], before),
            copy(g_ref.at[span(t)], next_g.at[span(t)], in_send_sem.at[2 * t + 1], in_recv_sem.at[2 * t + 1], before),
        )

    def stat_copy(t):
        return copy(stat_send.at[t], stat_recv.at[t], stat_send_sem.at[t], stat_recv_sem.at[t], after)

    def norm_copy(t):
        return copy(norm_send.at[t], norm_recv.at[t], norm_send_sem.at[t], norm_recv_sem.at[t], before)

    def dq_copy(t):
        return copy(dq_send.at[t], dq_recv.at[t], dq_send_sem.at[t], dq_recv_sem.at[t], after)

    def loop(count, body):
        def step(i, carry):
            body(i + 1)
            return carry

        lax.fori_loop(0, count - 1, step, 0)

    def sp_peer(k):
        return lax.rem(me + k, n_sp)

    def tp_peer(k):
        return lax.rem(me_tp + k, n_tp)

    barrier = pltpu.get_barrier_semaphore()

    def greet(target):
        pl.semaphore_signal(barrier, inc=1, device_id=target, device_id_type=MESH)

    loop(n_sp, lambda k: greet({"sp": sp_peer(k)}))
    loop(n_tp, lambda k: greet({"tp": tp_peer(k)}))
    moves = ((q_hbm, q_ref), (g_hbm, g_ref), (k_hbm, k_ref), (v_hbm, v_ref))
    loads = [pltpu.make_async_copy(a, b, load_sem.at[i]) for i, (a, b) in enumerate(moves)]
    moves = ((k_out, k_out_hbm), (v_out, v_out_hbm), (q_out, q_out_hbm))
    stores = [pltpu.make_async_copy(a, b, store_sem.at[i]) for i, (a, b) in enumerate(moves)]
    for c in loads:
        c.start()
    pl.semaphore_wait(barrier, n_sp + n_tp - 2)
    loads[0].wait()
    loads[1].wait()

    @pl.when(has_prev)
    def _():
        for t in range(tiles):
            for c in in_copies(t):
                c.start()

    loads[2].wait()
    loads[3].wait()
    q_gain = jnp.concatenate([q_gain_ref[...]] * 2, axis=1)
    k_gain = jnp.concatenate([k_gain_ref[...]] * 2, axis=1)
    low_lane = iota((TILE, LANES), 1) < LANES // 2

    def split_heads(x):
        first = jnp.where(low_lane, x, 0.0)
        second = jnp.where(low_lane, 0.0, x)
        return jnp.concatenate([first, second], axis=0).astype(jnp.bfloat16)

    def load_queries(q_from, g_from, t, q_to, g_to, unit_to, scale_to):
        for p in range(pairs):
            x = q_from[span(t), pair_lanes(p)].astype(jnp.float32)
            unit, scale = unit_of(x)
            unit_to[p, span(t)] = unit
            if scale_to is not None:
                scale_to[p, span(t)] = scale
            q_to[p, t] = split_heads(unit * q_gain)
            g_to[p, t] = split_heads(g_from[span(t), pair_lanes(p)].astype(jnp.float32))

    key_at = iota((TILE, WIDE), 0)
    query_at = iota((TILE, WIDE), 1) % TILE
    causal = query_at >= key_at
    far_bias = jnp.where((key_at // 64) >= (query_at // 64), 0.0, MASKED)

    for p in range(pairs):
        for t in range(tiles):
            x = k_ref[span(t), pair_lanes(p)].astype(jnp.float32)
            unit, scale = unit_of(x)
            k_unit[p, span(t)] = unit
            k_scale[p, span(t)] = scale
            hat = unit * k_gain
            k_hat[p, span(t)] = hat.astype(jnp.bfloat16)
            k_turned[p, :, span(t)] = hat.T.astype(jnp.bfloat16)
        sheets = []
        for h in (2 * p, 2 * p + 1):
            table = (bias_ref[h : h + 1, 0:CLIP] - bias_ref[h : h + 1, CLIP : CLIP + 1]) * LOG2E
            sheets.append(skew(jnp.broadcast_to(table, (TILE, LANES)), False))
        near_bias[p] = jnp.concatenate(sheets, axis=1)
    dk[...] = jnp.zeros_like(dk)
    dv[...] = jnp.zeros_like(dv)
    taps[...] = jnp.zeros_like(taps)
    totals[...] = jnp.zeros_like(totals)
    gain_part[...] = jnp.zeros_like(gain_part)

    def forward(p, t, start, stop, kinds, q_from, g_from, e_to, p_to):
        keys = slice(start * TILE, stop * TILE)
        raw = dot(k_hat[p, keys], q_from[p, t], NT)
        grad = dot(v_ref[keys, pair_lanes(p)], g_from[p, t], NT)
        total = jnp.zeros((1, WIDE), jnp.float32)
        inner = jnp.zeros((1, WIDE), jnp.float32)
        for c in range(start, stop):
            here = slice((c - start) * TILE, (c - start + 1) * TILE)
            s = raw[here] * (score_scale * LOG2E)
            kind = kinds.get(c)
            if kind == "diagonal":
                s = jnp.where(causal, s + near_bias[p], MASKED)
            elif kind == "below":
                s = s + jnp.where(causal, 0.0, near_bias[p])
            elif kind == "far":
                s = s + far_bias
            e = jnp.exp2(s)
            dp = grad[here]
            e_to[p, t, span(c)] = e
            p_to[p, t, span(c)] = dp
            total = total + jnp.sum(e, axis=0, keepdims=True)
            inner = inner + jnp.sum(e * dp, axis=0, keepdims=True)
        return total, inner

    def backward(p, t, start, stop, kinds, q_from, g_from, e_from, p_from, inverse, delta):
        keys = slice(start * TILE, stop * TILE)
        attention = e_from[p, t, keys] * inverse
        grad = attention * (p_from[p, t, keys] - delta)
        attention_low = attention.astype(jnp.bfloat16)
        grad_low = grad.astype(jnp.bfloat16)
        dv[p, keys] += dot(attention_low, g_from[p, t])
        dk[p, keys] += dot(grad_low, q_from[p, t])
        turned = dot(k_turned[p, :, keys], grad_low)
        totals[p : p + 1] += jnp.sum(grad, axis=0, keepdims=True)
        for c, kind in kinds.items():
            part = grad[(c - start) * TILE : (c - start + 1) * TILE]
            if kind == "diagonal":
                taps[p] += part
            elif kind == "below":
                taps[p] += jnp.where(causal, 0.0, part)
        upper = iota((LANES, TILE), 0) < LANES // 2
        return jnp.where(upper, turned[:, :TILE], turned[:, TILE:]).T

    def own_kinds(t):
        kinds = {t: "diagonal"}
        if t > 0:
            kinds[t - 1] = "below"
        return kinds

    def far_forward_kinds(t):
        kinds = {t: "far"}
        if t == 0:
            kinds[tiles - 1] = "below"
        return kinds

    for t in range(tiles):
        load_queries(q_ref, g_ref, t, own_q, own_g, q_unit, q_scale)
        for p in range(pairs):
            total, inner = forward(p, t, 0, t + 1, own_kinds(t), own_q, own_g, own_e, own_p)
            own_stat[t, 2 * p : 2 * p + 1] = total
            own_stat[t, 2 * p + 1 : 2 * p + 2] = inner

    def far_forward(t):
        @pl.when(has_next)
        def _():
            for c in in_copies(t):
                c.wait_recv()
            load_queries(next_q, next_g, t, far_q, far_g, next_unit, None)
            for p in range(pairs):
                total, inner = forward(
                    p, t, t, tiles, far_forward_kinds(t), far_q, far_g, far_e, far_p
                )
                stat_send[t, 2 * p : 2 * p + 1] = total
                stat_send[t, 2 * p + 1 : 2 * p + 2] = inner
            stat_copy(t).start()

    def own_backward(t):
        @pl.when(has_prev)
        def _():
            stat_copy(t).wait_recv()
            for p in range(pairs):
                total = own_stat[t, 2 * p : 2 * p + 1] + stat_recv[t, 2 * p : 2 * p + 1]
                inner = own_stat[t, 2 * p + 1 : 2 * p + 2] + stat_recv[t, 2 * p + 1 : 2 * p + 2]
                inverse = 1.0 / total
                norm_send[t, 2 * p : 2 * p + 1] = inverse
                norm_send[t, 2 * p + 1 : 2 * p + 2] = inner * inverse
            norm_copy(t).start()

        @pl.when(jnp.logical_not(has_prev))
        def _():
            for p in range(pairs):
                inverse = 1.0 / own_stat[t, 2 * p : 2 * p + 1]
                norm_send[t, 2 * p : 2 * p + 1] = inverse
                norm_send[t, 2 * p + 1 : 2 * p + 2] = own_stat[t, 2 * p + 1 : 2 * p + 2] * inverse

        for p in range(pairs):
            inverse = norm_send[t, 2 * p : 2 * p + 1]
            delta = norm_send[t, 2 * p + 1 : 2 * p + 2]
            part = backward(
                p, t, 0, t + 1, own_kinds(t), own_q, own_g, own_e, own_p, inverse, delta
            )
            dq_own[p, span(t)] = part
            gain_part[...] += jnp.sum(part * q_unit[p, span(t)], axis=0, keepdims=True)

    def far_backward(t):
        @pl.when(has_next)
        def _():
            norm_copy(t).wait_recv()
            for p in range(pairs):
                inverse = norm_recv[t, 2 * p : 2 * p + 1]
                delta = norm_recv[t, 2 * p + 1 : 2 * p + 2]
                part = backward(
                    p, t, t, tiles, far_forward_kinds(t), far_q, far_g, far_e, far_p, inverse, delta
                )
                dq_send[t, :, pair_lanes(p)] = part.astype(jnp.bfloat16)
                gain_part[...] += jnp.sum(part * next_unit[p, span(t)], axis=0, keepdims=True)
            dq_copy(t).start()

    for step in range(tiles + 1):
        if step < tiles:
            far_forward(step)
        if step >= 1:
            own_backward(step - 1)
    for t in range(tiles):
        far_backward(t)

    k_part = jnp.zeros((1, LANES), jnp.float32)
    for p in range(pairs):
        k_part = k_part + jnp.sum(dk[p] * k_unit[p], axis=0, keepdims=True)

    gain_row = message.shape[0] - 8
    message[...] = jnp.zeros_like(message)
    for h in range(heads):
        lanes = slice((h % 2) * TILE, (h % 2 + 1) * TILE)
        row = jnp.sum(skew(taps[h // 2, :, lanes], True), axis=0, keepdims=True)
        rest = jnp.sum(totals[h // 2 : h // 2 + 1, lanes], axis=1, keepdims=True) - jnp.sum(
            row, axis=1, keepdims=True
        )
        message[h : h + 1] = row
        message[heads + h : heads + h + 1] = jnp.broadcast_to(rest, (1, LANES))
    message[gain_row : gain_row + 1] = gain_part[...] * score_scale
    message[gain_row + 1 : gain_row + 2] = k_part * score_scale

    def sum_copy(k, slot, target):
        return copy(message, gathered.at[slot], sum_send_sem.at[k], sum_recv_sem.at[slot], target)

    loop(n_sp, lambda k: sum_copy(k, me, sp_peer(k)).start())
    gathered[me] = message[...]

    def norm_backward(unit, scale, grad_hat, gain):
        grad_unit = grad_hat * gain
        inner = half_mean(grad_unit * unit)
        return (scale * (grad_unit - unit * inner)).astype(jnp.bfloat16)

    for p in range(pairs):
        for t in range(tiles):
            here = (p, span(t))
            k_out[span(t), pair_lanes(p)] = norm_backward(
                k_unit[here], k_scale[here], dk[here] * score_scale, k_gain
            )
            v_out[span(t), pair_lanes(p)] = dv[here].astype(jnp.bfloat16)

    stores[0].start()
    stores[1].start()

    @pl.when(jnp.logical_not(has_prev))
    def _():
        dq_recv[...] = jnp.zeros_like(dq_recv)

    for t in range(tiles):

        @pl.when(has_prev)
        def _():
            dq_copy(t).wait_recv()

        for p in range(pairs):
            here = (p, span(t))
            grad_hat = (dq_own[here] + dq_recv[t, :, pair_lanes(p)].astype(jnp.float32)) * score_scale
            q_out[span(t), pair_lanes(p)] = norm_backward(
                q_unit[here], q_scale[here], grad_hat, q_gain
            )

    stores[2].start()
    loop(n_sp, lambda k: sum_copy(k, sp_peer(k), sp_peer(k)).wait_recv())
    summed = jnp.sum(gathered[...], axis=0)
    for h in range(heads):
        bias_out[h : h + 1, 0:CLIP] = summed[h : h + 1]
        bias_out[h : h + 1, CLIP : CLIP + 1] = summed[heads + h : heads + h + 1, 0:1]
    gain_message[...] = summed[gain_row:]

    def gain_copy(k, slot):
        return pltpu.make_async_remote_copy(
            src_ref=gain_message,
            dst_ref=gain_gathered.at[slot],
            send_sem=gain_send_sem.at[k],
            recv_sem=gain_recv_sem.at[slot],
            device_id={"tp": tp_peer(k)},
            device_id_type=MESH,
        )

    loop(n_tp, lambda k: gain_copy(k, me_tp).start())
    gain_gathered[me_tp] = gain_message[...]
    loop(n_tp, lambda k: gain_copy(k, tp_peer(k)).wait_recv())
    gains = jnp.sum(gain_gathered[...], axis=0)
    gains = gains + pltpu.roll(gains, LANES // 2, 1)
    q_gain_out[...] = gains[0:1, 0 : LANES // 2]
    k_gain_out[...] = gains[1:2, 0 : LANES // 2]

    for c in stores:
        c.wait()
    loop(n_sp, lambda k: sum_copy(k, me, sp_peer(k)).wait_send())
    loop(n_tp, lambda k: gain_copy(k, me_tp).wait_send())

    @pl.when(has_prev)
    def _():
        for t in range(tiles):
            for c in in_copies(t):
                c.wait_send()
            norm_copy(t).wait_send()

    @pl.when(has_next)
    def _():
        for t in range(tiles):
            stat_copy(t).wait_send()
            dq_copy(t).wait_send()


def place(*refs):
    half = len(refs) // 2
    for source, target in zip(refs[:half], refs[half:]):
        target[...] = source[...]


def per_device(axis_sizes, query, key, value, out_grad, query_gain, key_gain, rel_bias):
    n_sp, n_tp = axis_sizes
    rows, width = query.shape
    heads, taps = rel_bias.shape
    head_width = width // heads
    tiles = rows // TILE
    pairs = width // LANES
    low, full = jnp.bfloat16, jnp.float32
    message_rows = -(-2 * heads // 8) * 8 + 8
    stat_rows = -(-2 * pairs // 8) * 8
    vmem = pl.BlockSpec(memory_space=pltpu.VMEM)
    anywhere = pl.BlockSpec(memory_space=pl.ANY)
    stat = pltpu.VMEM((tiles, stat_rows, WIDE), full)
    wide = pltpu.VMEM((pairs, tiles, WIDE, LANES), low)
    square = pltpu.VMEM((pairs, tiles, rows, WIDE), full)
    units = pltpu.VMEM((pairs, rows, LANES), full)
    dma = pltpu.SemaphoreType.DMA
    results = pl.pallas_call(
        functools.partial(kernel, axis_sizes, head_width),
        out_shape=(
            jax.ShapeDtypeStruct((rows, width), low),
            jax.ShapeDtypeStruct((rows, width), low),
            jax.ShapeDtypeStruct((rows, width), low),
            jax.ShapeDtypeStruct((1, head_width), full),
            jax.ShapeDtypeStruct((1, head_width), full),
            jax.ShapeDtypeStruct((heads, taps), full),
        ),
        in_specs=[anywhere] * 4 + [vmem] * 3,
        out_specs=(anywhere,) * 3 + (vmem,) * 3,
        scratch_shapes=[pltpu.VMEM((rows, width), low)] * 7
        + [
            pltpu.VMEM((rows, width), low),
            pltpu.VMEM((rows, width), low),
            stat,
            stat,
            stat,
            stat,
            pltpu.VMEM((tiles, TILE, width), low),
            pltpu.VMEM((tiles, TILE, width), low),
            pltpu.VMEM((pairs, rows, LANES), low),
            pltpu.VMEM((pairs, LANES, rows), low),
            wide,
            wide,
            wide,
            wide,
            square,
            square,
            square,
            square,
            pltpu.VMEM((pairs, rows, LANES), full),
            pltpu.VMEM((pairs, rows, LANES), full),
            pltpu.VMEM((pairs, rows, LANES), full),
            pltpu.VMEM((pairs, TILE, WIDE), full),
            pltpu.VMEM((pairs, TILE, WIDE), full),
            pltpu.VMEM((8, WIDE), full),
            stat,
            units,
            units,
            units,
            units,
            units,
            pltpu.VMEM((1, LANES), full),
            pltpu.VMEM((message_rows, LANES), full),
            pltpu.VMEM((n_sp, message_rows, LANES), full),
            pltpu.VMEM((8, LANES), full),
            pltpu.VMEM((n_tp, 8, LANES), full),
            dma((2 * tiles,)),
            dma((2 * tiles,)),
            dma((tiles,)),
            dma((tiles,)),
            dma((tiles,)),
            dma((tiles,)),
            dma((tiles,)),
            dma((tiles,)),
            dma((n_sp,)),
            dma((n_sp,)),
            dma((n_tp,)),
            dma((n_tp,)),
            dma((4,)),
            dma((3,)),
        ],
        compiler_params=pltpu.CompilerParams(has_side_effects=True, collective_id=0),
    )(query, key, value, out_grad, query_gain.reshape(1, -1), key_gain.reshape(1, -1), rel_bias)
    query_grad, key_grad, value_grad, query_gain_grad, key_gain_grad, bias_grad = pl.pallas_call(
        place,
        out_shape=tuple(jax.ShapeDtypeStruct(x.shape, x.dtype) for x in results),
        in_specs=[vmem] * 6,
        out_specs=(vmem,) * 6,
    )(*results)
    return (
        query_grad,
        key_grad,
        value_grad,
        query_gain_grad.reshape(-1),
        key_gain_grad.reshape(-1),
        bias_grad,
    )


def solution(mesh):
    axis_sizes = (mesh.shape["sp"], mesh.shape["tp"])
    placed = (P("sp", "tp"), P("sp", "tp"), P("sp", "tp"), P("sp", "tp"), P(), P(), P("tp", None))
    return jax.shard_map(
        functools.partial(per_device, axis_sizes),
        mesh=mesh,
        in_specs=placed,
        out_specs=(P("sp", "tp"), P("sp", "tp"), P("sp", "tp"), P(), P(), P("tp", None)),
        check_vma=False,
    )
```

profile of v0, /device:TPU:0, one launch (start us, length us, event | category | flops | bytes accessed | tf_op | source)
XLA Modules:
  0.0 38.9 jit_solution(1799344307355490127)
XLA Ops:
  0.6 36.2 %shard_map.118 = (bf16[512,256]{1,0:T(8,128)(2,1)}, bf16[512,256]{1,0:T(8,128)(2,1)}, bf16[512,256]{1,0:T(8,128)(2,1)}, f32[1,64]{1,0:T(1,128)}, f32[1,64]{1,0:T(1,128)}, /*index=5*/f32[4,129]{1,0:T(4,128)}) custom-call(bf16[512,256]{1,0:T(8,128)(2,1)} %q_hbm.1, bf16[512,256]{1,0:T(8,128)(2,1)} %k_hbm.1, bf16[512,256]{1,0:T(8,128)(2,1)} %v_hbm.1, ...), custom_call_target="tpu_custom_call" | custom-call | tf_op jit(solution)/shard_map/pallas_call | solution.py:500
  36.8 2.0 %shard_map.119 = (bf16[512,256]{1,0:T(8,128)(2,1)}, bf16[512,256]{1,0:T(8,128)(2,1)}, bf16[512,256]{1,0:T(8,128)(2,1)}, f32[1,64]{1,0:T(1,128)}, f32[1,64]{1,0:T(1,128)}, /*index=5*/f32[4,129]{1,0:T(4,128)}) custom-call(bf16[512,256]{1,0:T(8,128)(2,1)} %get-tuple-element.18.refs_0_, bf16[512,256]{1,0:T(8,128)(2,1)} %get-tuple-element.19.refs_1_, ...), custom_call_target="tpu_custom_call" | custom-call | tf_op jit(solution)/shard_map/pallas_call | solution.py:566
where the time goes:
time: 39 us; the launch traced here: 38.9 us
  Pallas kernels  38.2 us (98%)
  between operations  0.64 us (2%)
    pallas_call x1, Pallas kernels, per_device(): pl.pallas_call(functools.partial(kernel, axis_sizes, head_width), out_sha...  36.2 us
    pallas_call x1, Pallas kernels, per_device(): pl.pallas_call(place, out_shape=tuple((jax.ShapeDtypeStruct(x.shape, x.dt...  2.02 us

commit v1 on v0

--- a/solution.py
+++ b/solution.py
@@ -75,8 +75,7 @@
     next_g,
     stat_send,
     stat_recv,
-    norm_send,
-    norm_recv,
+    next_stat,
     dq_send,
     dq_recv,
     k_hat,
@@ -110,8 +109,8 @@
     in_recv_sem,
     stat_send_sem,
     stat_recv_sem,
-    norm_send_sem,
-    norm_recv_sem,
+    own_send_sem,
+    own_recv_sem,
     dq_send_sem,
     dq_recv_sem,
     sum_send_sem,
@@ -159,8 +158,8 @@
     def stat_copy(t):
         return copy(stat_send.at[t], stat_recv.at[t], stat_send_sem.at[t], stat_recv_sem.at[t], after)
 
-    def norm_copy(t):
-        return copy(norm_send.at[t], norm_recv.at[t], norm_send_sem.at[t], norm_recv_sem.at[t], before)
+    def own_copy():
+        return copy(own_stat, next_stat, own_send_sem.at[0], own_recv_sem.at[0], before)
 
     def dq_copy(t):
         return copy(dq_send.at[t], dq_recv.at[t], dq_send_sem.at[t], dq_recv_sem.at[t], after)
@@ -195,11 +194,13 @@
     loads[0].wait()
     loads[1].wait()
 
+    in_order = [c for t in range(tiles) for c in in_copies(t)]
+    ahead = min(3, len(in_order))
+
     @pl.when(has_prev)
     def _():
-        for t in range(tiles):
-            for c in in_copies(t):
-                c.start()
+        for c in in_order[:ahead]:
+            c.start()
 
     loads[2].wait()
     loads[3].wait()
@@ -302,12 +303,34 @@
             kinds[tiles - 1] = "below"
         return kinds
 
+    def stat_row(p, t):
+        return 2 * (t * pairs + p)
+
+    def normalizers(p, t, own, far):
+        row = stat_row(p, t)
+        total = own[row : row + 1] + far[t, 2 * p : 2 * p + 1]
+        inner = own[row + 1 : row + 2] + far[t, 2 * p + 1 : 2 * p + 2]
+        inverse = 1.0 / total
+        return inverse, inner * inverse
+
     for t in range(tiles):
         load_queries(q_ref, g_ref, t, own_q, own_g, q_unit, q_scale)
         for p in range(pairs):
             total, inner = forward(p, t, 0, t + 1, own_kinds(t), own_q, own_g, own_e, own_p)
-            own_stat[t, 2 * p : 2 * p + 1] = total
-            own_stat[t, 2 * p + 1 : 2 * p + 2] = inner
+            row = stat_row(p, t)
+            own_stat[row : row + 1] = total
+            own_stat[row + 1 : row + 2] = inner
+
+    @pl.when(has_prev)
+    def _():
+        own_copy().start()
+        for c in in_order[ahead:]:
+            c.start()
+
+    @pl.when(jnp.logical_not(has_prev))
+    def _():
+        stat_recv[...] = jnp.zeros_like(stat_recv)
+        dq_recv[...] = jnp.zeros_like(dq_recv)
 
     def far_forward(t):
         @pl.when(has_next)
@@ -323,55 +346,47 @@
                 stat_send[t, 2 * p + 1 : 2 * p + 2] = inner
             stat_copy(t).start()
 
+    def far_backward(t):
+        @pl.when(has_next)
+        def _():
+            if t == 0:
+                own_copy().wait_recv()
+            for p in range(pairs):
+                inverse, delta = normalizers(p, t, next_stat, stat_send)
+                part = backward(
+                    p, t, t, tiles, far_forward_kinds(t), far_q, far_g, far_e, far_p, inverse, delta
+                )
+                dq_send[t, :, pair_lanes(p)] = part.astype(jnp.bfloat16)
+                gain_part[...] += jnp.sum(part * next_unit[p, span(t)], axis=0, keepdims=True)
+
+    def dq_start(ts):
+        @pl.when(has_next)
+        def _():
+            for t in ts:
+                dq_copy(t).start()
+
     def own_backward(t):
         @pl.when(has_prev)
         def _():
             stat_copy(t).wait_recv()
-            for p in range(pairs):
-                total = own_stat[t, 2 * p : 2 * p + 1] + stat_recv[t, 2 * p : 2 * p + 1]
-                inner = own_stat[t, 2 * p + 1 : 2 * p + 2] + stat_recv[t, 2 * p + 1 : 2 * p + 2]
-                inverse = 1.0 / total
-                norm_send[t, 2 * p : 2 * p + 1] = inverse
-                norm_send[t, 2 * p + 1 : 2 * p + 2] = inner * inverse
-            norm_copy(t).start()
-
-        @pl.when(jnp.logical_not(has_prev))
-        def _():
-            for p in range(pairs):
-                inverse = 1.0 / own_stat[t, 2 * p : 2 * p + 1]
-                norm_send[t, 2 * p : 2 * p + 1] = inverse
-                norm_send[t, 2 * p + 1 : 2 * p + 2] = own_stat[t, 2 * p + 1 : 2 * p + 2] * inverse
 
         for p in range(pairs):
-            inverse = norm_send[t, 2 * p : 2 * p + 1]
-            delta = norm_send[t, 2 * p + 1 : 2 * p + 2]
+            inverse, delta = normalizers(p, t, own_stat, stat_recv)
             part = backward(
                 p, t, 0, t + 1, own_kinds(t), own_q, own_g, own_e, own_p, inverse, delta
             )
             dq_own[p, span(t)] = part
             gain_part[...] += jnp.sum(part * q_unit[p, span(t)], axis=0, keepdims=True)
 
-    def far_backward(t):
-        @pl.when(has_next)
-        def _():
-            norm_copy(t).wait_recv()
-            for p in range(pairs):
-                inverse = norm_recv[t, 2 * p : 2 * p + 1]
-                delta = norm_recv[t, 2 * p + 1 : 2 * p + 2]
-                part = backward(
-                    p, t, t, tiles, far_forward_kinds(t), far_q, far_g, far_e, far_p, inverse, delta
-                )
-                dq_send[t, :, pair_lanes(p)] = part.astype(jnp.bfloat16)
-                gain_part[...] += jnp.sum(part * next_unit[p, span(t)], axis=0, keepdims=True)
-            dq_copy(t).start()
-
-    for step in range(tiles + 1):
-        if step < tiles:
-            far_forward(step)
-        if step >= 1:
-            own_backward(step - 1)
     for t in range(tiles):
-        far_backward(t)
+        far_forward(t)
+        if t < tiles - 1:
+            far_backward(t)
+    dq_start(range(tiles - 1))
+    far_backward(tiles - 1)
+    dq_start(range(tiles - 1, tiles))
+    for t in range(tiles):
+        own_backward(t)
 
     k_part = jnp.zeros((1, LANES), jnp.float32)
     for p in range(pairs):
@@ -412,10 +427,6 @@
     stores[0].start()
     stores[1].start()
 
-    @pl.when(jnp.logical_not(has_prev))
-    def _():
-        dq_recv[...] = jnp.zeros_like(dq_recv)
-
     for t in range(tiles):
 
         @pl.when(has_prev)
@@ -462,10 +473,9 @@
 
     @pl.when(has_prev)
     def _():
-        for t in range(tiles):
-            for c in in_copies(t):
-                c.wait_send()
-            norm_copy(t).wait_send()
+        own_copy().wait_send()
+        for c in in_order:
+            c.wait_send()
 
     @pl.when(has_next)
     def _():
@@ -493,6 +503,7 @@
     vmem = pl.BlockSpec(memory_space=pltpu.VMEM)
     anywhere = pl.BlockSpec(memory_space=pl.ANY)
     stat = pltpu.VMEM((tiles, stat_rows, WIDE), full)
+    sums = pltpu.VMEM((-(-2 * pairs * tiles // 8) * 8, WIDE), full)
     wide = pltpu.VMEM((pairs, tiles, WIDE, LANES), low)
     square = pltpu.VMEM((pairs, tiles, rows, WIDE), full)
     units = pltpu.VMEM((pairs, rows, LANES), full)
@@ -515,8 +526,7 @@
             pltpu.VMEM((rows, width), low),
             stat,
             stat,
-            stat,
-            stat,
+            sums,
             pltpu.VMEM((tiles, TILE, width), low),
             pltpu.VMEM((tiles, TILE, width), low),
             pltpu.VMEM((pairs, rows, LANES), low),
@@ -535,7 +545,7 @@
             pltpu.VMEM((pairs, TILE, WIDE), full),
             pltpu.VMEM((pairs, TILE, WIDE), full),
             pltpu.VMEM((8, WIDE), full),
-            stat,
+            sums,
             units,
             units,
             units,
@@ -550,8 +560,8 @@
             dma((2 * tiles,)),
             dma((tiles,)),
             dma((tiles,)),
-            dma((tiles,)),
-            dma((tiles,)),
+            dma((1,)),
+            dma((1,)),
             dma((tiles,)),
             dma((tiles,)),
             dma((n_sp,)),

time: 39 us -> 34.5 us (0.88)
  Pallas kernels: 38.2 us -> 33.6 us
    pallas_call x1, Pallas kernels: 36.2 us -> 31.6 us  [per_device(): pl.pallas_call(functools.partial(kernel, axis_sizes, head_width), out_sha...]
where the time goes in v1:
time: 34.5 us; the launch traced here: 34.3 us
  Pallas kernels  33.6 us (97%)
  between operations  0.64 us (2%)
    pallas_call x1, Pallas kernels, per_device(): pl.pallas_call(functools.partial(kernel, axis_sizes, head_width), out_sha...  31.6 us
    pallas_call x1, Pallas kernels, per_device(): pl.pallas_call(place, out_shape=tuple((jax.ShapeDtypeStruct(x.shape, x.dt...  2.02 us

profile of v1, /device:TPU:0, one launch (start us, length us, event | category | flops | bytes accessed | tf_op | source)
XLA Modules:
  0.0 34.3 jit_solution(7747169594446936689)
XLA Ops:
  0.6 31.6 %shard_map.118 = (bf16[512,256]{1,0:T(8,128)(2,1)}, bf16[512,256]{1,0:T(8,128)(2,1)}, bf16[512,256]{1,0:T(8,128)(2,1)}, f32[1,64]{1,0:T(1,128)}, f32[1,64]{1,0:T(1,128)}, /*index=5*/f32[4,129]{1,0:T(4,128)}) custom-call(bf16[512,256]{1,0:T(8,128)(2,1)} %q_hbm.1, bf16[512,256]{1,0:T(8,128)(2,1)} %k_hbm.1, bf16[512,256]{1,0:T(8,128)(2,1)} %v_hbm.1, ...), custom_call_target="tpu_custom_call" | custom-call | tf_op jit(solution)/shard_map/pallas_call | solution.py:511
  32.3 2.0 %shard_map.119 = (bf16[512,256]{1,0:T(8,128)(2,1)}, bf16[512,256]{1,0:T(8,128)(2,1)}, bf16[512,256]{1,0:T(8,128)(2,1)}, f32[1,64]{1,0:T(1,128)}, f32[1,64]{1,0:T(1,128)}, /*index=5*/f32[4,129]{1,0:T(4,128)}) custom-call(bf16[512,256]{1,0:T(8,128)(2,1)} %get-tuple-element.18.refs_0_, bf16[512,256]{1,0:T(8,128)(2,1)} %get-tuple-element.19.refs_1_, ...), custom_call_target="tpu_custom_call" | custom-call | tf_op jit(solution)/shard_map/pallas_call | solution.py:576

commit v2 on v1

--- a/solution.py
+++ b/solution.py
@@ -14,6 +14,8 @@
 EPSILON = 1e-06
 LOG2E = 1.4426950408889634
 MASKED = -1e30
+MAIN_VMEM = 48 * 1024 * 1024
+PLACE_VMEM = 4 * 1024 * 1024
 MESH = pl.DeviceIdType.MESH
 NT = (((1,), (1,)), ((), ()))
 NN = (((1,), (0,)), ((), ()))
@@ -55,12 +57,12 @@
     k_hbm,
     v_hbm,
     g_hbm,
-    q_gain_ref,
-    k_gain_ref,
-    bias_ref,
-    q_out_hbm,
-    k_out_hbm,
-    v_out_hbm,
+    q_gain_hbm,
+    k_gain_hbm,
+    bias_hbm,
+    q_out,
+    k_out,
+    v_out,
     q_gain_out,
     k_gain_out,
     bias_out,
@@ -68,9 +70,9 @@
     k_ref,
     v_ref,
     g_ref,
-    q_out,
-    k_out,
-    v_out,
+    q_gain_ref,
+    k_gain_ref,
+    bias_ref,
     next_q,
     next_g,
     stat_send,
@@ -118,7 +120,7 @@
     gain_send_sem,
     gain_recv_sem,
     load_sem,
-    store_sem,
+    met_sem,
 ):
     n_sp, n_tp = axis_sizes
     rows, width = q_hbm.shape
@@ -177,20 +179,55 @@
     def tp_peer(k):
         return lax.rem(me_tp + k, n_tp)
 
+    everyone = n_sp * n_tp
+    me_flat = me * n_tp + me_tp
+
+    def flat_peer(k):
+        return lax.rem(me_flat + k, everyone)
+
     barrier = pltpu.get_barrier_semaphore()
 
     def greet(target):
         pl.semaphore_signal(barrier, inc=1, device_id=target, device_id_type=MESH)
 
-    loop(n_sp, lambda k: greet({"sp": sp_peer(k)}))
+    pl.when(has_prev)(lambda: greet({"sp": before}))
+    pl.when(has_next)(lambda: greet({"sp": after}))
     loop(n_tp, lambda k: greet({"tp": tp_peer(k)}))
-    moves = ((q_hbm, q_ref), (g_hbm, g_ref), (k_hbm, k_ref), (v_hbm, v_ref))
+    moves = (
+        (q_hbm, q_ref),
+        (g_hbm, g_ref),
+        (k_hbm, k_ref),
+        (v_hbm, v_ref),
+        (q_gain_hbm, q_gain_ref),
+        (k_gain_hbm, k_gain_ref),
+        (bias_hbm, bias_ref),
+    )
     loads = [pltpu.make_async_copy(a, b, load_sem.at[i]) for i, (a, b) in enumerate(moves)]
-    moves = ((k_out, k_out_hbm), (v_out, v_out_hbm), (q_out, q_out_hbm))
-    stores = [pltpu.make_async_copy(a, b, store_sem.at[i]) for i, (a, b) in enumerate(moves)]
     for c in loads:
         c.start()
-    pl.semaphore_wait(barrier, n_sp + n_tp - 2)
+    pl.semaphore_wait(barrier, has_prev.astype(jnp.int32) + has_next.astype(jnp.int32) + n_tp - 1)
+    rounds = met_sem.shape[0]
+
+    def round_signal(r):
+        for ok, target in ((me >= 1 << r, me - (1 << r)), (me + (1 << r) < n_sp, me + (1 << r))):
+
+            @pl.when(ok)
+            def _():
+                pl.semaphore_signal(
+                    met_sem.at[r], inc=1, device_id={"sp": target}, device_id_type=MESH
+                )
+
+    def round_wait(r):
+        count = (me >= 1 << r).astype(jnp.int32) + (me + (1 << r) < n_sp).astype(jnp.int32)
+        pl.semaphore_wait(met_sem.at[r], count)
+
+    def meet(r):
+        if r < rounds:
+            round_wait(r)
+        if r + 1 < rounds:
+            round_signal(r + 1)
+
+    round_signal(0)
     loads[0].wait()
     loads[1].wait()
 
@@ -202,8 +239,8 @@
         for c in in_order[:ahead]:
             c.start()
 
-    loads[2].wait()
-    loads[3].wait()
+    for c in loads[2:]:
+        c.wait()
     q_gain = jnp.concatenate([q_gain_ref[...]] * 2, axis=1)
     k_gain = jnp.concatenate([k_gain_ref[...]] * 2, axis=1)
     low_lane = iota((TILE, LANES), 1) < LANES // 2
@@ -332,6 +369,8 @@
         stat_recv[...] = jnp.zeros_like(stat_recv)
         dq_recv[...] = jnp.zeros_like(dq_recv)
 
+    meet(0)
+
     def far_forward(t):
         @pl.when(has_next)
         def _():
@@ -382,9 +421,13 @@
         far_forward(t)
         if t < tiles - 1:
             far_backward(t)
+        if t == min(1, tiles - 1):
+            meet(1)
     dq_start(range(tiles - 1))
     far_backward(tiles - 1)
     dq_start(range(tiles - 1, tiles))
+    for r in range(2, rounds):
+        meet(r)
     for t in range(tiles):
         own_backward(t)
 
@@ -392,8 +435,25 @@
     for p in range(pairs):
         k_part = k_part + jnp.sum(dk[p] * k_unit[p], axis=0, keepdims=True)
 
-    gain_row = message.shape[0] - 8
-    message[...] = jnp.zeros_like(message)
+    halves = [x + pltpu.roll(x, LANES // 2, 1) for x in (gain_part[...], k_part)]
+    first_half = iota((1, LANES), 1) < LANES // 2
+    gain_message[...] = jnp.where(first_half, halves[0], halves[1]) * score_scale
+
+    def gain_copy(k, slot, target):
+        return pltpu.make_async_remote_copy(
+            src_ref=gain_message,
+            dst_ref=gain_gathered.at[slot],
+            send_sem=gain_send_sem.at[k],
+            recv_sem=gain_recv_sem.at[slot],
+            device_id={"sp": target // n_tp, "tp": lax.rem(target, n_tp)},
+            device_id_type=MESH,
+        )
+
+    loop(everyone, lambda k: gain_copy(k, me_flat, flat_peer(k)).start())
+    gain_gathered[me_flat] = gain_message[...]
+
+    if message.shape[0] > 2 * heads:
+        message[...] = jnp.zeros_like(message)
     for h in range(heads):
         lanes = slice((h % 2) * TILE, (h % 2 + 1) * TILE)
         row = jnp.sum(skew(taps[h // 2, :, lanes], True), axis=0, keepdims=True)
@@ -402,8 +462,6 @@
         )
         message[h : h + 1] = row
         message[heads + h : heads + h + 1] = jnp.broadcast_to(rest, (1, LANES))
-    message[gain_row : gain_row + 1] = gain_part[...] * score_scale
-    message[gain_row + 1 : gain_row + 2] = k_part * score_scale
 
     def sum_copy(k, slot, target):
         return copy(message, gathered.at[slot], sum_send_sem.at[k], sum_recv_sem.at[slot], target)
@@ -424,8 +482,6 @@
             )
             v_out[span(t), pair_lanes(p)] = dv[here].astype(jnp.bfloat16)
 
-    stores[0].start()
-    stores[1].start()
 
     for t in range(tiles):
 
@@ -440,36 +496,18 @@
                 q_unit[here], q_scale[here], grad_hat, q_gain
             )
 
-    stores[2].start()
     loop(n_sp, lambda k: sum_copy(k, sp_peer(k), sp_peer(k)).wait_recv())
     summed = jnp.sum(gathered[...], axis=0)
     for h in range(heads):
         bias_out[h : h + 1, 0:CLIP] = summed[h : h + 1]
         bias_out[h : h + 1, CLIP : CLIP + 1] = summed[heads + h : heads + h + 1, 0:1]
-    gain_message[...] = summed[gain_row:]
-
-    def gain_copy(k, slot):
-        return pltpu.make_async_remote_copy(
-            src_ref=gain_message,
-            dst_ref=gain_gathered.at[slot],
-            send_sem=gain_send_sem.at[k],
-            recv_sem=gain_recv_sem.at[slot],
-            device_id={"tp": tp_peer(k)},
-            device_id_type=MESH,
-        )
-
-    loop(n_tp, lambda k: gain_copy(k, me_tp).start())
-    gain_gathered[me_tp] = gain_message[...]
-    loop(n_tp, lambda k: gain_copy(k, tp_peer(k)).wait_recv())
+    loop(everyone, lambda k: gain_copy(k, flat_peer(k), flat_peer(k)).wait_recv())
     gains = jnp.sum(gain_gathered[...], axis=0)
-    gains = gains + pltpu.roll(gains, LANES // 2, 1)
-    q_gain_out[...] = gains[0:1, 0 : LANES // 2]
-    k_gain_out[...] = gains[1:2, 0 : LANES // 2]
-
-    for c in stores:
-        c.wait()
+    q_gain_out[...] = gains[:, 0 : LANES // 2]
+    k_gain_out[...] = gains[:, LANES // 2 :]
+
     loop(n_sp, lambda k: sum_copy(k, me, sp_peer(k)).wait_send())
-    loop(n_tp, lambda k: gain_copy(k, me_tp).wait_send())
+    loop(everyone, lambda k: gain_copy(k, me_flat, flat_peer(k)).wait_send())
 
     @pl.when(has_prev)
     def _():
@@ -486,8 +524,15 @@
 
 def place(*refs):
     half = len(refs) // 2
-    for source, target in zip(refs[:half], refs[half:]):
-        target[...] = source[...]
+    sem = refs[-1]
+    moves = [
+        pltpu.make_async_copy(source, target, sem.at[i])
+        for i, (source, target) in enumerate(zip(refs[:half], refs[half:-1]))
+    ]
+    for c in moves:
+        c.start()
+    for c in moves:
+        c.wait()
 
 
 def per_device(axis_sizes, query, key, value, out_grad, query_gain, key_gain, rel_bias):
@@ -498,7 +543,7 @@
     tiles = rows // TILE
     pairs = width // LANES
     low, full = jnp.bfloat16, jnp.float32
-    message_rows = -(-2 * heads // 8) * 8 + 8
+    message_rows = -(-2 * heads // 8) * 8
     stat_rows = -(-2 * pairs // 8) * 8
     vmem = pl.BlockSpec(memory_space=pltpu.VMEM)
     anywhere = pl.BlockSpec(memory_space=pl.ANY)
@@ -508,19 +553,26 @@
     square = pltpu.VMEM((pairs, tiles, rows, WIDE), full)
     units = pltpu.VMEM((pairs, rows, LANES), full)
     dma = pltpu.SemaphoreType.DMA
-    results = pl.pallas_call(
+    results = (
+        ((rows, width), low),
+        ((rows, width), low),
+        ((rows, width), low),
+        ((1, head_width), full),
+        ((1, head_width), full),
+        ((heads, taps), full),
+    )
+    given = (query, key, value, out_grad, query_gain.reshape(1, -1), key_gain.reshape(1, -1), rel_bias)
+    kept = pl.pallas_call(
         functools.partial(kernel, axis_sizes, head_width),
-        out_shape=(
-            jax.ShapeDtypeStruct((rows, width), low),
-            jax.ShapeDtypeStruct((rows, width), low),
-            jax.ShapeDtypeStruct((rows, width), low),
-            jax.ShapeDtypeStruct((1, head_width), full),
-            jax.ShapeDtypeStruct((1, head_width), full),
-            jax.ShapeDtypeStruct((heads, taps), full),
-        ),
-        in_specs=[anywhere] * 4 + [vmem] * 3,
-        out_specs=(anywhere,) * 3 + (vmem,) * 3,
-        scratch_shapes=[pltpu.VMEM((rows, width), low)] * 7
+        out_shape=tuple(pltpu.VMEM(shape, kind) for shape, kind in results),
+        in_specs=[anywhere] * 7,
+        out_specs=(vmem,) * 6,
+        scratch_shapes=[pltpu.VMEM((rows, width), low)] * 4
+        + [
+            pltpu.VMEM((1, head_width), full),
+            pltpu.VMEM((1, head_width), full),
+            pltpu.VMEM((heads, taps), full),
+        ]
         + [
             pltpu.VMEM((rows, width), low),
             pltpu.VMEM((rows, width), low),
@@ -554,8 +606,8 @@
             pltpu.VMEM((1, LANES), full),
             pltpu.VMEM((message_rows, LANES), full),
             pltpu.VMEM((n_sp, message_rows, LANES), full),
-            pltpu.VMEM((8, LANES), full),
-            pltpu.VMEM((n_tp, 8, LANES), full),
+            pltpu.VMEM((1, LANES), full),
+            pltpu.VMEM((n_sp * n_tp, 1, LANES), full),
             dma((2 * tiles,)),
             dma((2 * tiles,)),
             dma((tiles,)),
@@ -566,19 +618,23 @@
             dma((tiles,)),
             dma((n_sp,)),
             dma((n_sp,)),
-            dma((n_tp,)),
-            dma((n_tp,)),
-            dma((4,)),
-            dma((3,)),
+            dma((n_sp * n_tp,)),
+            dma((n_sp * n_tp,)),
+            dma((7,)),
+            pltpu.SemaphoreType.REGULAR((max((n_sp - 1).bit_length(), 1),)),
         ],
-        compiler_params=pltpu.CompilerParams(has_side_effects=True, collective_id=0),
-    )(query, key, value, out_grad, query_gain.reshape(1, -1), key_gain.reshape(1, -1), rel_bias)
+        compiler_params=pltpu.CompilerParams(
+            has_side_effects=True, collective_id=0, vmem_limit_bytes=MAIN_VMEM
+        ),
+    )(*(pltpu.with_memory_space_constraint(x, pltpu.HBM) for x in given))
     query_grad, key_grad, value_grad, query_gain_grad, key_gain_grad, bias_grad = pl.pallas_call(
         place,
-        out_shape=tuple(jax.ShapeDtypeStruct(x.shape, x.dtype) for x in results),
+        out_shape=tuple(jax.ShapeDtypeStruct(shape, kind) for shape, kind in results),
         in_specs=[vmem] * 6,
-        out_specs=(vmem,) * 6,
-    )(*results)
+        out_specs=(anywhere,) * 6,
+        scratch_shapes=[dma((6,))],
+        compiler_params=pltpu.CompilerParams(vmem_limit_bytes=PLACE_VMEM),
+    )(*kept)
     return (
         query_grad,
         key_grad,

time: 34.5 us -> 31.7 us (0.919)
  Pallas kernels: 33.6 us -> 31 us
    pallas_call x1, Pallas kernels: 31.6 us -> 30 us  [per_device(): pl.pallas_call(functools.partial(kernel, axis_sizes, head_width), out_sha...]
    pallas_call x1, Pallas kernels: 2.02 us -> 0.94 us  [per_device(): pl.pallas_call(place, out_shape=tuple((jax.ShapeDtypeStruct(shape, kind)...]
where the time goes in v2:
time: 31.7 us; the launch traced here: 31.6 us
  Pallas kernels  31 us (98%)
  between operations  0.64 us (2%)
    pallas_call x1, Pallas kernels, per_device(): pl.pallas_call(functools.partial(kernel, axis_sizes, head_width), out_sha...  30 us
    pallas_call x1, Pallas kernels, per_device(): pl.pallas_call(place, out_shape=tuple((jax.ShapeDtypeStruct(shape, kind)...  0.94 us

profile of v2, /device:TPU:0, one launch (start us, length us, event | category | flops | bytes accessed | tf_op | source)
XLA Modules:
  0.0 31.6 jit_solution(5758800316476307005)
XLA Ops:
  0.6 30.0 %shard_map.118 = (bf16[512,256]{1,0:T(8,128)(2,1)S(1)}, bf16[512,256]{1,0:T(8,128)(2,1)S(1)}, bf16[512,256]{1,0:T(8,128)(2,1)S(1)}, f32[1,64]{1,0:T(1,128)S(1)},...) custom-call(bf16[512,256]{1,0:T(8,128)(2,1)} %q_hbm.1, bf16[512,256]{1,0:T(8,128)(2,1)} %k_hbm.1, bf16[512,256]{1,0:T(8,128)(2,1)} %v_hbm.1, ...), custom_call_target="tpu_custom_call" | custom-call | tf_op jit(solution)/shard_map/pallas_call | solution.py:565
  30.7 0.9 %shard_map.119 = (bf16[512,256]{1,0:T(8,128)(2,1)}, bf16[512,256]{1,0:T(8,128)(2,1)}, bf16[512,256]{1,0:T(8,128)(2,1)}, f32[1,64]{1,0:T(1,128)}, f32[1,64]{1,0:T(1,128)}, /*index=5*/f32[4,129]{1,0:T(4,128)}) custom-call(bf16[512,256]{1,0:T(8,128)(2,1)S(1)} %get-tuple-element.18.refs_0_, bf16[512,256]{1,0:T(8,128)(2,1)S(1)} %get-tuple-element.19.refs_1_, ...), custom_call_target="tpu_custom_call" | custom-call | tf_op jit(solution)/shard_map/pallas_call | solution.py:630

commit v3 on v2

--- a/solution.py
+++ b/solution.py
@@ -41,13 +41,26 @@
     return x * scale, scale
 
 
-def skew(x, left):
+def low_skew(x, left):
     row = iota(x.shape, 0)
-    for bit in range(7):
+    for bit in range(3):
         step = 1 << bit
         moved = pltpu.roll(x, LANES - step if left else step, 1)
         x = jnp.where((row & step) != 0, moved, x)
     return x
+
+
+def by_distance(table):
+    first = low_skew(jnp.broadcast_to(table, (8, LANES)), False)
+    blocks = [first] + [pltpu.roll(first, at, 1) for at in range(8, TILE, 8)]
+    return jnp.concatenate(blocks, axis=0)
+
+
+def distance_sums(x):
+    total = x[0:8]
+    for at in range(8, TILE, 8):
+        total = total + pltpu.roll(x[at : at + 8], LANES - at, 1)
+    return jnp.sum(low_skew(total, True), axis=0, keepdims=True)
 
 
 def kernel(
@@ -75,6 +88,14 @@
     bias_ref,
     next_q,
     next_g,
+    prev_k,
+    prev_v,
+    prev_hat,
+    prev_turned,
+    prev_unit,
+    side_send,
+    side_recv,
+    k_gain_part,
     stat_send,
     stat_recv,
     next_stat,
@@ -121,10 +142,15 @@
     gain_recv_sem,
     load_sem,
     met_sem,
+    kv_send_sem,
+    kv_recv_sem,
+    side_send_sem,
+    side_recv_sem,
 ):
     n_sp, n_tp = axis_sizes
     rows, width = q_hbm.shape
     tiles = rows // TILE
+    last = tiles - 1
     pairs = width // LANES
     heads = 2 * pairs
     score_scale = head_width ** (-0.5)
@@ -165,6 +191,15 @@
 
     def dq_copy(t):
         return copy(dq_send.at[t], dq_recv.at[t], dq_send_sem.at[t], dq_recv_sem.at[t], after)
+
+    def kv_copies():
+        return (
+            copy(k_ref.at[span(last)], prev_k, kv_send_sem.at[0], kv_recv_sem.at[0], after),
+            copy(v_ref.at[span(last)], prev_v, kv_send_sem.at[1], kv_recv_sem.at[1], after),
+        )
+
+    def side_copy():
+        return copy(side_send, side_recv, side_send_sem.at[0], side_recv_sem.at[0], before)
 
     def loop(count, body):
         def step(i, carry):
@@ -231,7 +266,7 @@
     loads[0].wait()
     loads[1].wait()
 
-    in_order = [c for t in range(tiles) for c in in_copies(t)]
+    in_order = [c for t in range(last) for c in in_copies(t)]
     ahead = min(3, len(in_order))
 
     @pl.when(has_prev)
@@ -264,6 +299,8 @@
     query_at = iota((TILE, WIDE), 1) % TILE
     causal = query_at >= key_at
     far_bias = jnp.where((key_at // 64) >= (query_at // 64), 0.0, MASKED)
+
+    edge_bias = far_bias + jnp.where(has_prev, 0.0, MASKED)
 
     for p in range(pairs):
         for t in range(tiles):
@@ -277,13 +314,14 @@
         sheets = []
         for h in (2 * p, 2 * p + 1):
             table = (bias_ref[h : h + 1, 0:CLIP] - bias_ref[h : h + 1, CLIP : CLIP + 1]) * LOG2E
-            sheets.append(skew(jnp.broadcast_to(table, (TILE, LANES)), False))
+            sheets.append(by_distance(table))
         near_bias[p] = jnp.concatenate(sheets, axis=1)
     dk[...] = jnp.zeros_like(dk)
     dv[...] = jnp.zeros_like(dv)
     taps[...] = jnp.zeros_like(taps)
     totals[...] = jnp.zeros_like(totals)
     gain_part[...] = jnp.zeros_like(gain_part)
+    k_gain_part[...] = jnp.zeros_like(k_gain_part)
 
     def forward(p, t, start, stop, kinds, q_from, g_from, e_to, p_to):
         keys = slice(start * TILE, stop * TILE)
@@ -325,6 +363,9 @@
                 taps[p] += part
             elif kind == "below":
                 taps[p] += jnp.where(causal, 0.0, part)
+        return turned_back(turned)
+
+    def turned_back(turned):
         upper = iota((LANES, TILE), 0) < LANES // 2
         return jnp.where(upper, turned[:, :TILE], turned[:, TILE:]).T
 
@@ -367,7 +408,13 @@
     @pl.when(jnp.logical_not(has_prev))
     def _():
         stat_recv[...] = jnp.zeros_like(stat_recv)
+        prev_k[...] = jnp.zeros_like(prev_k)
+        prev_v[...] = jnp.zeros_like(prev_v)
         dq_recv[...] = jnp.zeros_like(dq_recv)
+
+    @pl.when(jnp.logical_not(has_next))
+    def _():
+        side_recv[...] = jnp.zeros_like(side_recv)
 
     meet(0)
 
@@ -404,10 +451,57 @@
             for t in ts:
                 dq_copy(t).start()
 
-    def own_backward(t):
+    def side_forward(t):
         @pl.when(has_prev)
         def _():
-            stat_copy(t).wait_recv()
+            for c in kv_copies():
+                c.wait_recv()
+
+        for p in range(pairs):
+            unit, _ = unit_of(prev_k[:, pair_lanes(p)].astype(jnp.float32))
+            prev_unit[p] = unit
+            hat = unit * k_gain
+            prev_hat[p] = hat.astype(jnp.bfloat16)
+            prev_turned[p] = hat.T.astype(jnp.bfloat16)
+            raw = dot(prev_hat[p], own_q[p, t], NT)
+            dp = dot(prev_v[:, pair_lanes(p)], own_g[p, t], NT)
+            e = jnp.exp2(raw * (score_scale * LOG2E) + edge_bias)
+            far_e[p, t, span(t)] = e
+            far_p[p, t, span(t)] = dp
+            stat_recv[t, 2 * p : 2 * p + 1] = jnp.sum(e, axis=0, keepdims=True)
+            stat_recv[t, 2 * p + 1 : 2 * p + 2] = jnp.sum(e * dp, axis=0, keepdims=True)
+
+    def side_backward(t):
+        for p in range(pairs):
+            inverse, delta = normalizers(p, t, own_stat, stat_recv)
+            attention = far_e[p, t, span(t)] * inverse
+            grad = attention * (far_p[p, t, span(t)] - delta)
+            attention_low = attention.astype(jnp.bfloat16)
+            grad_low = grad.astype(jnp.bfloat16)
+            dk_part = dot(grad_low, own_q[p, t])
+            side_send[0, :, pair_lanes(p)] = dk_part.astype(jnp.bfloat16)
+            side_send[1, :, pair_lanes(p)] = dot(attention_low, own_g[p, t]).astype(jnp.bfloat16)
+            k_gain_part[...] += jnp.sum(dk_part * prev_unit[p], axis=0, keepdims=True)
+            totals[p : p + 1] += jnp.sum(grad, axis=0, keepdims=True)
+            part = turned_back(dot(prev_turned[p], grad_low))
+            dq_own[p, span(t)] += part
+            gain_part[...] += jnp.sum(part * q_unit[p, span(t)], axis=0, keepdims=True)
+
+    def kv_start():
+        @pl.when(has_next)
+        def _():
+            for c in kv_copies():
+                c.start()
+
+    def side_start():
+        pl.when(has_prev)(lambda: side_copy().start())
+
+    def own_backward(t):
+        if t < last:
+
+            @pl.when(has_prev)
+            def _():
+                stat_copy(t).wait_recv()
 
         for p in range(pairs):
             inverse, delta = normalizers(p, t, own_stat, stat_recv)
@@ -417,21 +511,25 @@
             dq_own[p, span(t)] = part
             gain_part[...] += jnp.sum(part * q_unit[p, span(t)], axis=0, keepdims=True)
 
-    for t in range(tiles):
+    for t in range(last):
         far_forward(t)
-        if t < tiles - 1:
-            far_backward(t)
-        if t == min(1, tiles - 1):
+        far_backward(t)
+        if t == max(last - 2, 0):
+            kv_start()
+        if t == min(1, last):
             meet(1)
-    dq_start(range(tiles - 1))
-    far_backward(tiles - 1)
-    dq_start(range(tiles - 1, tiles))
     for r in range(2, rounds):
         meet(r)
-    for t in range(tiles):
+    early = max(last - 1, 0)
+    dq_start(range(early))
+    for t in range(last - 1):
         own_backward(t)
-
-    k_part = jnp.zeros((1, LANES), jnp.float32)
+    side_forward(last)
+    own_backward(last)
+    side_backward(last)
+    own_backward(last - 1)
+
+    k_part = k_gain_part[...]
     for p in range(pairs):
         k_part = k_part + jnp.sum(dk[p] * k_unit[p], axis=0, keepdims=True)
 
@@ -439,87 +537,113 @@
     first_half = iota((1, LANES), 1) < LANES // 2
     gain_message[...] = jnp.where(first_half, halves[0], halves[1]) * score_scale
 
-    def gain_copy(k, slot, target):
+    def gain_copy(slot, target):
         return pltpu.make_async_remote_copy(
             src_ref=gain_message,
             dst_ref=gain_gathered.at[slot],
-            send_sem=gain_send_sem.at[k],
-            recv_sem=gain_recv_sem.at[slot],
+            send_sem=gain_send_sem.at[0],
+            recv_sem=gain_recv_sem.at[0],
             device_id={"sp": target // n_tp, "tp": lax.rem(target, n_tp)},
             device_id_type=MESH,
         )
 
-    loop(everyone, lambda k: gain_copy(k, me_flat, flat_peer(k)).start())
+    loop(everyone, lambda k: gain_copy(me_flat, flat_peer(k)).start())
     gain_gathered[me_flat] = gain_message[...]
 
     if message.shape[0] > 2 * heads:
         message[...] = jnp.zeros_like(message)
     for h in range(heads):
         lanes = slice((h % 2) * TILE, (h % 2 + 1) * TILE)
-        row = jnp.sum(skew(taps[h // 2, :, lanes], True), axis=0, keepdims=True)
+        row = distance_sums(taps[h // 2, :, lanes])
         rest = jnp.sum(totals[h // 2 : h // 2 + 1, lanes], axis=1, keepdims=True) - jnp.sum(
             row, axis=1, keepdims=True
         )
         message[h : h + 1] = row
         message[heads + h : heads + h + 1] = jnp.broadcast_to(rest, (1, LANES))
 
-    def sum_copy(k, slot, target):
-        return copy(message, gathered.at[slot], sum_send_sem.at[k], sum_recv_sem.at[slot], target)
-
-    loop(n_sp, lambda k: sum_copy(k, me, sp_peer(k)).start())
+    def sum_copy(slot, target):
+        return copy(message, gathered.at[slot], sum_send_sem.at[0], sum_recv_sem.at[0], target)
+
+    loop(n_sp, lambda k: sum_copy(me, sp_peer(k)).start())
     gathered[me] = message[...]
+    dq_start(range(early, last))
+    side_start()
 
     def norm_backward(unit, scale, grad_hat, gain):
         grad_unit = grad_hat * gain
         inner = half_mean(grad_unit * unit)
         return (scale * (grad_unit - unit * inner)).astype(jnp.bfloat16)
 
-    for p in range(pairs):
-        for t in range(tiles):
+    def finish_keys(t, dk_more, dv_more):
+        for p in range(pairs):
             here = (p, span(t))
+            dk_all, dv_all = dk[here], dv[here]
+            if dk_more is not None:
+                dk_all = dk_all + dk_more[:, pair_lanes(p)].astype(jnp.float32)
+                dv_all = dv_all + dv_more[:, pair_lanes(p)].astype(jnp.float32)
             k_out[span(t), pair_lanes(p)] = norm_backward(
-                k_unit[here], k_scale[here], dk[here] * score_scale, k_gain
+                k_unit[here], k_scale[here], dk_all * score_scale, k_gain
             )
-            v_out[span(t), pair_lanes(p)] = dv[here].astype(jnp.bfloat16)
-
-
-    for t in range(tiles):
+            v_out[span(t), pair_lanes(p)] = dv_all.astype(jnp.bfloat16)
+
+    def finish_queries(t, dq_more):
+        for p in range(pairs):
+            here = (p, span(t))
+            dq_all = dq_own[here]
+            if dq_more is not None:
+                dq_all = dq_all + dq_more[:, pair_lanes(p)].astype(jnp.float32)
+            q_out[span(t), pair_lanes(p)] = norm_backward(
+                q_unit[here], q_scale[here], dq_all * score_scale, q_gain
+            )
+
+    for t in range(last):
+        finish_keys(t, None, None)
+    finish_queries(last, None)
+    for t in range(last):
 
         @pl.when(has_prev)
         def _():
             dq_copy(t).wait_recv()
 
-        for p in range(pairs):
-            here = (p, span(t))
-            grad_hat = (dq_own[here] + dq_recv[t, :, pair_lanes(p)].astype(jnp.float32)) * score_scale
-            q_out[span(t), pair_lanes(p)] = norm_backward(
-                q_unit[here], q_scale[here], grad_hat, q_gain
-            )
-
-    loop(n_sp, lambda k: sum_copy(k, sp_peer(k), sp_peer(k)).wait_recv())
+        finish_queries(t, dq_recv.at[t])
+
+    @pl.when(has_next)
+    def _():
+        side_copy().wait_recv()
+
+    finish_keys(last, side_recv.at[0], side_recv.at[1])
+    def drain():
+        @pl.when(has_prev)
+        def _():
+            own_copy().wait_send()
+            side_copy().wait_send()
+            for c in in_order:
+                c.wait_send()
+
+        @pl.when(has_next)
+        def _():
+            for c in kv_copies():
+                c.wait_send()
+            for t in range(last):
+                stat_copy(t).wait_send()
+                dq_copy(t).wait_send()
+
+    all_sums = gathered.at[0 : n_sp - 1]
+    all_sums = copy(all_sums, all_sums, sum_send_sem.at[0], sum_recv_sem.at[0], before)
+    all_gains = gain_gathered.at[0 : everyone - 1]
+    all_gains = copy(all_gains, all_gains, gain_send_sem.at[0], gain_recv_sem.at[0], before)
+    all_sums.wait_send()
+    all_gains.wait_send()
+    drain()
+    all_sums.wait_recv()
     summed = jnp.sum(gathered[...], axis=0)
     for h in range(heads):
         bias_out[h : h + 1, 0:CLIP] = summed[h : h + 1]
         bias_out[h : h + 1, CLIP : CLIP + 1] = summed[heads + h : heads + h + 1, 0:1]
-    loop(everyone, lambda k: gain_copy(k, flat_peer(k), flat_peer(k)).wait_recv())
+    all_gains.wait_recv()
     gains = jnp.sum(gain_gathered[...], axis=0)
     q_gain_out[...] = gains[:, 0 : LANES // 2]
     k_gain_out[...] = gains[:, LANES // 2 :]
-
-    loop(n_sp, lambda k: sum_copy(k, me, sp_peer(k)).wait_send())
-    loop(everyone, lambda k: gain_copy(k, me_flat, flat_peer(k)).wait_send())
-
-    @pl.when(has_prev)
-    def _():
-        own_copy().wait_send()
-        for c in in_order:
-            c.wait_send()
-
-    @pl.when(has_next)
-    def _():
-        for t in range(tiles):
-            stat_copy(t).wait_send()
-            dq_copy(t).wait_send()
 
 
 def place(*refs):
@@ -576,6 +700,14 @@
         + [
             pltpu.VMEM((rows, width), low),
             pltpu.VMEM((rows, width), low),
+            pltpu.VMEM((TILE, width), low),
+            pltpu.VMEM((TILE, width), low),
+            pltpu.VMEM((pairs, TILE, LANES), low),
+            pltpu.VMEM((pairs, LANES, TILE), low),
+            pltpu.VMEM((pairs, TILE, LANES), full),
+            pltpu.VMEM((2, TILE, width), low),
+            pltpu.VMEM((2, TILE, width), low),
+            pltpu.VMEM((1, LANES), full),
             stat,
             stat,
             sums,
@@ -616,12 +748,16 @@
             dma((1,)),
             dma((tiles,)),
             dma((tiles,)),
-            dma((n_sp,)),
-            dma((n_sp,)),
-            dma((n_sp * n_tp,)),
-            dma((n_sp * n_tp,)),
+            dma((1,)),
+            dma((1,)),
+            dma((1,)),
+            dma((1,)),
             dma((7,)),
             pltpu.SemaphoreType.REGULAR((max((n_sp - 1).bit_length(), 1),)),
+            dma((2,)),
+            dma((2,)),
+            dma((1,)),
+            dma((1,)),
         ],
         compiler_params=pltpu.CompilerParams(
             has_side_effects=True, collective_id=0, vmem_limit_bytes=MAIN_VMEM

time: 31.7 us -> 28.7 us (0.905)
  Pallas kernels: 31 us -> 28 us
    pallas_call x1, Pallas kernels: 30 us -> 27 us  [per_device(): pl.pallas_call(functools.partial(kernel, axis_sizes, head_width), out_sha...]
where the time goes in v3:
time: 28.7 us; the launch traced here: 28.6 us
  Pallas kernels  28 us (98%)
  between operations  0.64 us (2%)
    pallas_call x1, Pallas kernels, per_device(): pl.pallas_call(functools.partial(kernel, axis_sizes, head_width), out_sha...  27 us
    pallas_call x1, Pallas kernels, per_device(): pl.pallas_call(place, out_shape=tuple((jax.ShapeDtypeStruct(shape, kind)...  0.94 us

profile of v3, /device:TPU:0, one launch (start us, length us, event | category | flops | bytes accessed | tf_op | source)
XLA Modules:
  0.0 28.6 jit_solution(3724432502026307502)
XLA Ops:
  0.6 27.0 %shard_map.118 = (bf16[512,256]{1,0:T(8,128)(2,1)S(1)}, bf16[512,256]{1,0:T(8,128)(2,1)S(1)}, bf16[512,256]{1,0:T(8,128)(2,1)S(1)}, f32[1,64]{1,0:T(1,128)S(1)},...) custom-call(bf16[512,256]{1,0:T(8,128)(2,1)} %q_hbm.1, bf16[512,256]{1,0:T(8,128)(2,1)} %k_hbm.1, bf16[512,256]{1,0:T(8,128)(2,1)} %v_hbm.1, ...), custom_call_target="tpu_custom_call" | custom-call | tf_op jit(solution)/shard_map/pallas_call | solution.py:689
  27.7 0.9 %shard_map.119 = (bf16[512,256]{1,0:T(8,128)(2,1)}, bf16[512,256]{1,0:T(8,128)(2,1)}, bf16[512,256]{1,0:T(8,128)(2,1)}, f32[1,64]{1,0:T(1,128)}, f32[1,64]{1,0:T(1,128)}, /*index=5*/f32[4,129]{1,0:T(4,128)}) custom-call(bf16[512,256]{1,0:T(8,128)(2,1)S(1)} %get-tuple-element.18.refs_0_, bf16[512,256]{1,0:T(8,128)(2,1)S(1)} %get-tuple-element.19.refs_1_, ...), custom_call_target="tpu_custom_call" | custom-call | tf_op jit(solution)/shard_map/pallas_call | solution.py:766

commit v4 on v3

--- a/solution.py
+++ b/solution.py
@@ -79,17 +79,13 @@
     q_gain_out,
     k_gain_out,
     bias_out,
-    q_ref,
-    k_ref,
-    v_ref,
-    g_ref,
+    qg_ref,
+    kv_ref,
     q_gain_ref,
     k_gain_ref,
     bias_ref,
-    next_q,
-    next_g,
-    prev_k,
-    prev_v,
+    next_qg,
+    prev_kv,
     prev_hat,
     prev_turned,
     prev_unit,
@@ -161,6 +157,11 @@
     before = jnp.maximum(me - 1, 0)
     after = jnp.minimum(me + 1, n_sp - 1)
 
+    q_ref, g_ref = qg_ref.at[0], qg_ref.at[1]
+    k_ref, v_ref = kv_ref.at[0], kv_ref.at[1]
+    next_q, next_g = next_qg.at[0], next_qg.at[1]
+    prev_k, prev_v = prev_kv.at[0], prev_kv.at[1]
+
     def span(t):
         return slice(t * TILE, (t + 1) * TILE)
 
@@ -177,10 +178,9 @@
             device_id_type=MESH,
         )
 
-    def in_copies(t):
-        return (
-            copy(q_ref.at[span(t)], next_q.at[span(t)], in_send_sem.at[2 * t], in_recv_sem.at[2 * t], before),
-            copy(g_ref.at[span(t)], next_g.at[span(t)], in_send_sem.at[2 * t + 1], in_recv_sem.at[2 * t + 1], before),
+    def in_copy(t):
+        return copy(
+            qg_ref.at[:, span(t)], next_qg.at[:, span(t)], in_send_sem.at[t], in_recv_sem.at[t], before
         )
 
     def stat_copy(t):
@@ -192,11 +192,8 @@
     def dq_copy(t):
         return copy(dq_send.at[t], dq_recv.at[t], dq_send_sem.at[t], dq_recv_sem.at[t], after)
 
-    def kv_copies():
-        return (
-            copy(k_ref.at[span(last)], prev_k, kv_send_sem.at[0], kv_recv_sem.at[0], after),
-            copy(v_ref.at[span(last)], prev_v, kv_send_sem.at[1], kv_recv_sem.at[1], after),
-        )
+    def kv_copy():
+        return copy(kv_ref.at[:, span(last)], prev_kv, kv_send_sem.at[0], kv_recv_sem.at[0], after)
 
     def side_copy():
         return copy(side_send, side_recv, side_send_sem.at[0], side_recv_sem.at[0], before)
@@ -227,7 +224,7 @@
 
     pl.when(has_prev)(lambda: greet({"sp": before}))
     pl.when(has_next)(lambda: greet({"sp": after}))
-    loop(n_tp, lambda k: greet({"tp": tp_peer(k)}))
+    pl.when(me == 0)(lambda: loop(n_tp, lambda k: greet({"tp": tp_peer(k)})))
     moves = (
         (q_hbm, q_ref),
         (g_hbm, g_ref),
@@ -240,8 +237,9 @@
     loads = [pltpu.make_async_copy(a, b, load_sem.at[i]) for i, (a, b) in enumerate(moves)]
     for c in loads:
         c.start()
-    pl.semaphore_wait(barrier, has_prev.astype(jnp.int32) + has_next.astype(jnp.int32) + n_tp - 1)
-    rounds = met_sem.shape[0]
+    neighbours = has_prev.astype(jnp.int32) + has_next.astype(jnp.int32)
+    pl.semaphore_wait(barrier, neighbours + jnp.where(me == 0, n_tp - 1, 0))
+    rounds = met_sem.shape[0] - 2
 
     def round_signal(r):
         for ok, target in ((me >= 1 << r, me - (1 << r)), (me + (1 << r) < n_sp, me + (1 << r))):
@@ -262,12 +260,37 @@
         if r + 1 < rounds:
             round_signal(r + 1)
 
+    def column_met():
+        @pl.when(me == 0)
+        def _():
+            def tell(k):
+                pl.semaphore_signal(
+                    met_sem.at[rounds], inc=1, device_id={"tp": tp_peer(k)}, device_id_type=MESH
+                )
+
+            loop(n_tp, tell)
+
+    def all_met():
+        @pl.when(me == 0)
+        def _():
+            pl.semaphore_wait(met_sem.at[rounds], n_tp - 1)
+
+            def tell(k):
+                pl.semaphore_signal(
+                    met_sem.at[rounds + 1], inc=1, device_id={"sp": k}, device_id_type=MESH
+                )
+
+            loop(n_sp, tell)
+
+    def round_end():
+        pl.when(me > 0)(lambda: pl.semaphore_wait(met_sem.at[rounds + 1], 1))
+
     round_signal(0)
     loads[0].wait()
     loads[1].wait()
 
-    in_order = [c for t in range(last) for c in in_copies(t)]
-    ahead = min(3, len(in_order))
+    in_order = [in_copy(t) for t in range(last)]
+    ahead = min(1, last)
 
     @pl.when(has_prev)
     def _():
@@ -408,8 +431,7 @@
     @pl.when(jnp.logical_not(has_prev))
     def _():
         stat_recv[...] = jnp.zeros_like(stat_recv)
-        prev_k[...] = jnp.zeros_like(prev_k)
-        prev_v[...] = jnp.zeros_like(prev_v)
+        prev_kv[...] = jnp.zeros_like(prev_kv)
         dq_recv[...] = jnp.zeros_like(dq_recv)
 
     @pl.when(jnp.logical_not(has_next))
@@ -421,8 +443,7 @@
     def far_forward(t):
         @pl.when(has_next)
         def _():
-            for c in in_copies(t):
-                c.wait_recv()
+            in_copy(t).wait_recv()
             load_queries(next_q, next_g, t, far_q, far_g, next_unit, None)
             for p in range(pairs):
                 total, inner = forward(
@@ -454,8 +475,7 @@
     def side_forward(t):
         @pl.when(has_prev)
         def _():
-            for c in kv_copies():
-                c.wait_recv()
+            kv_copy().wait_recv()
 
         for p in range(pairs):
             unit, _ = unit_of(prev_k[:, pair_lanes(p)].astype(jnp.float32))
@@ -488,13 +508,10 @@
             gain_part[...] += jnp.sum(part * q_unit[p, span(t)], axis=0, keepdims=True)
 
     def kv_start():
-        @pl.when(has_next)
-        def _():
-            for c in kv_copies():
-                c.start()
-
-    def side_start():
-        pl.when(has_prev)(lambda: side_copy().start())
+        pl.when(has_next)(lambda: kv_copy().start())
+
+    def side_start(odd):
+        pl.when(has_prev & (lax.rem(me, 2) == odd))(lambda: side_copy().start())
 
     def own_backward(t):
         if t < last:
@@ -516,19 +533,23 @@
         far_backward(t)
         if t == max(last - 2, 0):
             kv_start()
-        if t == min(1, last):
-            meet(1)
-    for r in range(2, rounds):
+        if t < last - 1:
+            meet(t + 1)
+    for r in range(last, rounds):
         meet(r)
+    column_met()
     early = max(last - 1, 0)
-    dq_start(range(early))
     for t in range(last - 1):
         own_backward(t)
+    all_met()
+    dq_start(range(early))
     side_forward(last)
     own_backward(last)
     side_backward(last)
+    side_start(1)
     own_backward(last - 1)
 
+    round_end()
     k_part = k_gain_part[...]
     for p in range(pairs):
         k_part = k_part + jnp.sum(dk[p] * k_unit[p], axis=0, keepdims=True)
@@ -547,7 +568,14 @@
             device_id_type=MESH,
         )
 
-    loop(everyone, lambda k: gain_copy(me_flat, flat_peer(k)).start())
+    def gain_start(k):
+        gain_copy(me_flat, flat_peer(k)).start()
+
+    if everyone <= 64:
+        for k in range(1, everyone):
+            gain_start(k)
+    else:
+        loop(everyone, gain_start)
     gain_gathered[me_flat] = gain_message[...]
 
     if message.shape[0] > 2 * heads:
@@ -567,7 +595,7 @@
     loop(n_sp, lambda k: sum_copy(me, sp_peer(k)).start())
     gathered[me] = message[...]
     dq_start(range(early, last))
-    side_start()
+    side_start(0)
 
     def norm_backward(unit, scale, grad_hat, gain):
         grad_unit = grad_hat * gain
@@ -622,8 +650,7 @@
 
         @pl.when(has_next)
         def _():
-            for c in kv_copies():
-                c.wait_send()
+            kv_copy().wait_send()
             for t in range(last):
                 stat_copy(t).wait_send()
                 dq_copy(t).wait_send()
@@ -691,17 +718,15 @@
         out_shape=tuple(pltpu.VMEM(shape, kind) for shape, kind in results),
         in_specs=[anywhere] * 7,
         out_specs=(vmem,) * 6,
-        scratch_shapes=[pltpu.VMEM((rows, width), low)] * 4
+        scratch_shapes=[pltpu.VMEM((2, rows, width), low)] * 2
         + [
             pltpu.VMEM((1, head_width), full),
             pltpu.VMEM((1, head_width), full),
             pltpu.VMEM((heads, taps), full),
         ]
         + [
-            pltpu.VMEM((rows, width), low),
-            pltpu.VMEM((rows, width), low),
-            pltpu.VMEM((TILE, width), low),
-            pltpu.VMEM((TILE, width), low),
+            pltpu.VMEM((2, rows, width), low),
+            pltpu.VMEM((2, TILE, width), low),
             pltpu.VMEM((pairs, TILE, LANES), low),
             pltpu.VMEM((pairs, LANES, TILE), low),
             pltpu.VMEM((pairs, TILE, LANES), full),
@@ -740,22 +765,22 @@
             pltpu.VMEM((n_sp, message_rows, LANES), full),
             pltpu.VMEM((1, LANES), full),
             pltpu.VMEM((n_sp * n_tp, 1, LANES), full),
-            dma((2 * tiles,)),
-            dma((2 * tiles,)),
             dma((tiles,)),
             dma((tiles,)),
-            dma((1,)),
-            dma((1,)),
             dma((tiles,)),
             dma((tiles,)),
             dma((1,)),
             dma((1,)),
+            dma((tiles,)),
+            dma((tiles,)),
+            dma((1,)),
+            dma((1,)),
             dma((1,)),
             dma((1,)),
             dma((7,)),
-            pltpu.SemaphoreType.REGULAR((max((n_sp - 1).bit_length(), 1),)),
-            dma((2,)),
-            dma((2,)),
+            pltpu.SemaphoreType.REGULAR((max((n_sp - 1).bit_length(), 1) + 2,)),
+            dma((1,)),
+            dma((1,)),
             dma((1,)),
             dma((1,)),
         ],

time: 28.7 us -> 27.8 us (0.969)
  Pallas kernels: 28 us -> 27 us
    pallas_call x1, Pallas kernels: 27 us -> 26.1 us  [per_device(): pl.pallas_call(functools.partial(kernel, axis_sizes, head_width), out_sha...]
where the time goes in v4:
time: 27.8 us; the launch traced here: 27.7 us
  Pallas kernels  27 us (97%)
  between operations  0.64 us (2%)
    pallas_call x1, Pallas kernels, per_device(): pl.pallas_call(functools.partial(kernel, axis_sizes, head_width), out_sha...  26.1 us
    pallas_call x1, Pallas kernels, per_device(): pl.pallas_call(place, out_shape=tuple((jax.ShapeDtypeStruct(shape, kind)...  0.94 us

profile of v4, /device:TPU:0, one launch (start us, length us, event | category | flops | bytes accessed | tf_op | source)
XLA Modules:
  0.0 27.7 jit_solution(2257835085087976678)
XLA Ops:
  0.6 26.1 %shard_map.118 = (bf16[512,256]{1,0:T(8,128)(2,1)S(1)}, bf16[512,256]{1,0:T(8,128)(2,1)S(1)}, bf16[512,256]{1,0:T(8,128)(2,1)S(1)}, f32[1,64]{1,0:T(1,128)S(1)},...) custom-call(bf16[512,256]{1,0:T(8,128)(2,1)} %q_hbm.1, bf16[512,256]{1,0:T(8,128)(2,1)} %k_hbm.1, bf16[512,256]{1,0:T(8,128)(2,1)} %v_hbm.1, ...), custom_call_target="tpu_custom_call" | custom-call | tf_op jit(solution)/shard_map/pallas_call | solution.py:716
  26.7 0.9 %shard_map.119 = (bf16[512,256]{1,0:T(8,128)(2,1)}, bf16[512,256]{1,0:T(8,128)(2,1)}, bf16[512,256]{1,0:T(8,128)(2,1)}, f32[1,64]{1,0:T(1,128)}, f32[1,64]{1,0:T(1,128)}, /*index=5*/f32[4,129]{1,0:T(4,128)}) custom-call(bf16[512,256]{1,0:T(8,128)(2,1)S(1)} %get-tuple-element.18.refs_0_, bf16[512,256]{1,0:T(8,128)(2,1)S(1)} %get-tuple-element.19.refs_1_, ...), custom_call_target="tpu_custom_call" | custom-call | tf_op jit(solution)/shard_map/pallas_call | solution.py:791

commit v5 on v4

--- a/solution.py
+++ b/solution.py
@@ -86,12 +86,8 @@
     bias_ref,
     next_qg,
     prev_kv,
-    prev_hat,
-    prev_turned,
-    prev_unit,
     side_send,
     side_recv,
-    k_gain_part,
     stat_send,
     stat_recv,
     next_stat,
@@ -344,7 +340,6 @@
     taps[...] = jnp.zeros_like(taps)
     totals[...] = jnp.zeros_like(totals)
     gain_part[...] = jnp.zeros_like(gain_part)
-    k_gain_part[...] = jnp.zeros_like(k_gain_part)
 
     def forward(p, t, start, stop, kinds, q_from, g_from, e_to, p_to):
         keys = slice(start * TILE, stop * TILE)
@@ -479,33 +474,21 @@
 
         for p in range(pairs):
             unit, _ = unit_of(prev_k[:, pair_lanes(p)].astype(jnp.float32))
-            prev_unit[p] = unit
+            k_unit[p, span(tiles)] = unit
             hat = unit * k_gain
-            prev_hat[p] = hat.astype(jnp.bfloat16)
-            prev_turned[p] = hat.T.astype(jnp.bfloat16)
-            raw = dot(prev_hat[p], own_q[p, t], NT)
+            k_turned[p, :, span(tiles)] = hat.T.astype(jnp.bfloat16)
+            raw = dot(hat.astype(jnp.bfloat16), own_q[p, t], NT)
             dp = dot(prev_v[:, pair_lanes(p)], own_g[p, t], NT)
             e = jnp.exp2(raw * (score_scale * LOG2E) + edge_bias)
-            far_e[p, t, span(t)] = e
-            far_p[p, t, span(t)] = dp
+            own_e[p, t, span(tiles)] = e
+            own_p[p, t, span(tiles)] = dp
             stat_recv[t, 2 * p : 2 * p + 1] = jnp.sum(e, axis=0, keepdims=True)
             stat_recv[t, 2 * p + 1 : 2 * p + 2] = jnp.sum(e * dp, axis=0, keepdims=True)
 
-    def side_backward(t):
+    def side_pack():
         for p in range(pairs):
-            inverse, delta = normalizers(p, t, own_stat, stat_recv)
-            attention = far_e[p, t, span(t)] * inverse
-            grad = attention * (far_p[p, t, span(t)] - delta)
-            attention_low = attention.astype(jnp.bfloat16)
-            grad_low = grad.astype(jnp.bfloat16)
-            dk_part = dot(grad_low, own_q[p, t])
-            side_send[0, :, pair_lanes(p)] = dk_part.astype(jnp.bfloat16)
-            side_send[1, :, pair_lanes(p)] = dot(attention_low, own_g[p, t]).astype(jnp.bfloat16)
-            k_gain_part[...] += jnp.sum(dk_part * prev_unit[p], axis=0, keepdims=True)
-            totals[p : p + 1] += jnp.sum(grad, axis=0, keepdims=True)
-            part = turned_back(dot(prev_turned[p], grad_low))
-            dq_own[p, span(t)] += part
-            gain_part[...] += jnp.sum(part * q_unit[p, span(t)], axis=0, keepdims=True)
+            side_send[0, :, pair_lanes(p)] = dk[p, span(tiles)].astype(jnp.bfloat16)
+            side_send[1, :, pair_lanes(p)] = dv[p, span(tiles)].astype(jnp.bfloat16)
 
     def kv_start():
         pl.when(has_next)(lambda: kv_copy().start())
@@ -520,10 +503,11 @@
             def _():
                 stat_copy(t).wait_recv()
 
+        stop = t + 1 if t < last else tiles + 1
         for p in range(pairs):
             inverse, delta = normalizers(p, t, own_stat, stat_recv)
             part = backward(
-                p, t, 0, t + 1, own_kinds(t), own_q, own_g, own_e, own_p, inverse, delta
+                p, t, 0, stop, own_kinds(t), own_q, own_g, own_e, own_p, inverse, delta
             )
             dq_own[p, span(t)] = part
             gain_part[...] += jnp.sum(part * q_unit[p, span(t)], axis=0, keepdims=True)
@@ -545,12 +529,12 @@
     dq_start(range(early))
     side_forward(last)
     own_backward(last)
-    side_backward(last)
+    side_pack()
     side_start(1)
     own_backward(last - 1)
 
     round_end()
-    k_part = k_gain_part[...]
+    k_part = jnp.zeros((1, LANES), jnp.float32)
     for p in range(pairs):
         k_part = k_part + jnp.sum(dk[p] * k_unit[p], axis=0, keepdims=True)
 
@@ -701,8 +685,9 @@
     stat = pltpu.VMEM((tiles, stat_rows, WIDE), full)
     sums = pltpu.VMEM((-(-2 * pairs * tiles // 8) * 8, WIDE), full)
     wide = pltpu.VMEM((pairs, tiles, WIDE, LANES), low)
-    square = pltpu.VMEM((pairs, tiles, rows, WIDE), full)
+    square = pltpu.VMEM((pairs, tiles, rows + TILE, WIDE), full)
     units = pltpu.VMEM((pairs, rows, LANES), full)
+    more_units = pltpu.VMEM((pairs, rows + TILE, LANES), full)
     dma = pltpu.SemaphoreType.DMA
     results = (
         ((rows, width), low),
@@ -727,19 +712,15 @@
         + [
             pltpu.VMEM((2, rows, width), low),
             pltpu.VMEM((2, TILE, width), low),
-            pltpu.VMEM((pairs, TILE, LANES), low),
-            pltpu.VMEM((pairs, LANES, TILE), low),
-            pltpu.VMEM((pairs, TILE, LANES), full),
             pltpu.VMEM((2, TILE, width), low),
             pltpu.VMEM((2, TILE, width), low),
-            pltpu.VMEM((1, LANES), full),
             stat,
             stat,
             sums,
             pltpu.VMEM((tiles, TILE, width), low),
             pltpu.VMEM((tiles, TILE, width), low),
             pltpu.VMEM((pairs, rows, LANES), low),
-            pltpu.VMEM((pairs, LANES, rows), low),
+            pltpu.VMEM((pairs, LANES, rows + TILE), low),
             wide,
             wide,
             wide,
@@ -748,9 +729,9 @@
             square,
             square,
             square,
-            pltpu.VMEM((pairs, rows, LANES), full),
-            pltpu.VMEM((pairs, rows, LANES), full),
-            pltpu.VMEM((pairs, rows, LANES), full),
+            more_units,
+            more_units,
+            units,
             pltpu.VMEM((pairs, TILE, WIDE), full),
             pltpu.VMEM((pairs, TILE, WIDE), full),
             pltpu.VMEM((8, WIDE), full),
@@ -758,7 +739,7 @@
             units,
             units,
             units,
-            units,
+            more_units,
             units,
             pltpu.VMEM((1, LANES), full),
             pltpu.VMEM((message_rows, LANES), full),

time: 27.8 us -> 27.8 us (level)
  no operation moved by 1% of the time
where the time goes in v5:
time: 27.8 us; the launch traced here: 27.7 us
  Pallas kernels  27 us (97%)
  between operations  0.64 us (2%)
    pallas_call x1, Pallas kernels, per_device(): pl.pallas_call(functools.partial(kernel, axis_sizes, head_width), out_sha...  26.1 us
    pallas_call x1, Pallas kernels, per_device(): pl.pallas_call(place, out_shape=tuple((jax.ShapeDtypeStruct(shape, kind)...  0.94 us

profile of v5, /device:TPU:0, one launch (start us, length us, event | category | flops | bytes accessed | tf_op | source)
XLA Modules:
  0.0 27.7 jit_solution(1773002757055725519)
XLA Ops:
  0.6 26.1 %shard_map.118 = (bf16[512,256]{1,0:T(8,128)(2,1)S(1)}, bf16[512,256]{1,0:T(8,128)(2,1)S(1)}, bf16[512,256]{1,0:T(8,128)(2,1)S(1)}, f32[1,64]{1,0:T(1,128)S(1)},...) custom-call(bf16[512,256]{1,0:T(8,128)(2,1)} %q_hbm.1, bf16[512,256]{1,0:T(8,128)(2,1)} %k_hbm.1, bf16[512,256]{1,0:T(8,128)(2,1)} %v_hbm.1, ...), custom_call_target="tpu_custom_call" | custom-call | tf_op jit(solution)/shard_map/pallas_call | solution.py:701
  26.7 0.9 %shard_map.119 = (bf16[512,256]{1,0:T(8,128)(2,1)}, bf16[512,256]{1,0:T(8,128)(2,1)}, bf16[512,256]{1,0:T(8,128)(2,1)}, f32[1,64]{1,0:T(1,128)}, f32[1,64]{1,0:T(1,128)}, /*index=5*/f32[4,129]{1,0:T(4,128)}) custom-call(bf16[512,256]{1,0:T(8,128)(2,1)S(1)} %get-tuple-element.18.refs_0_, bf16[512,256]{1,0:T(8,128)(2,1)S(1)} %get-tuple-element.19.refs_1_, ...), custom_call_target="tpu_custom_call" | custom-call | tf_op jit(solution)/shard_map/pallas_call | solution.py:772
